TPU v7x, 32 devices: a whole 2x2x4 slice. The times are simulated.
32 devices in a mesh: ep: 8 (over z, x), tp: 4 (over y, core).
Axes of the slice: x: 2, y: 2, z: 4, core: 2. Of those that a mesh axis runs over, the one named last changes fastest.
Arguments:
- query_logits: bfloat16 [2048, 2048], P('ep', 'tp'), may hold values from -6 to 6
- forget_gate_logits: bfloat16 [2048, 2048], P('ep', 'tp'), may hold values from -3.75 to 3.75
- written_values: bfloat16 [2048, 2048], P('ep', 'tp'), may hold values from -6 to 6
- output_gate_logits: bfloat16 [2048, 2048], P('ep', 'tp'), may hold values from -6 to 6
- gap: float32 [2048], P('tp'), may hold values from 4.8828125e-05 to 0.06
- extra_log_forget: float32 [2048, 2048], P('ep', 'tp'), may hold values from -0.7 to 0
- head_norm_scale: float32 [2048], P('tp'), may hold values from 0.1 to 1.9
- mixer_output_matrix: bfloat16 [2048, 2048], P('tp'), may hold values from -0.125 to 0.125
- expert_input_tokens: bfloat16 [2048, 2048], P('ep'), may hold values from -12 to 12
- expert_norm_scale: float32 [2048], replicated, may hold values from 0.1 to 1.9
- routes: int32 [2048, 2], P('ep'), may hold values from 0 to 7, all different within a row; in each aligned block of 256 rows (0 to 255, 256 to 511, ...) at most 96 rows name the same one
- router_scores_chosen: float32 [2048, 2], P('ep'), may hold values from -6 to 6
- expert_gate_matrix: bfloat16 [8, 2048, 4096], P('ep', None, 'tp'), may hold values from -0.125 to 0.125
- expert_up_matrix: bfloat16 [8, 2048, 4096], P('ep', None, 'tp'), may hold values from -0.125 to 0.125
- expert_down_matrix: bfloat16 [8, 2048, 4096], P('ep', None, 'tp'), may hold values from -0.09375 to 0.09375
Outputs:
- mixer_output_rows: bfloat16 [2048, 2048], P(('ep', 'tp'))
- expert_out: bfloat16 [2048, 2048], P('ep', 'tp')
Inputs may be any that keep to these rules, and one draw needn't show every extreme that they name: `routes`: each row names two different experts. Among the rows of one device no expert is named more than 96 times, and 96 is reached in some blocks.
All inputs are finite; a program needn't handle non-finite values.
Results may differ from a plain program's by a relative error of at most 0.019.
Values may be sent and summed in bfloat16 or wider, within the bound.
No kernel may reach another device: no remote copies, remote signals or barrier semaphores. Data moves between devices by JAX's collectives and lax.ppermute only.
A program may use at most 64 MiB of HBM per device.

v0:
```python
import jax
import jax.numpy as jnp
from jax import lax
from jax.sharding import PartitionSpec as P

HEAD_DIM = 128


exact_precision = lax.Precision.HIGHEST


def entering(x, axis, join, neutral):
    place = lax.axis_index(axis)
    gathered = jax.tree.map(
        lambda a, kind: lax.all_gather(a.astype(kind), axis), x, (jnp.bfloat16, jnp.bfloat16)
    )
    state = jax.tree.map(lambda a, e: jnp.zeros_like(a) + jnp.asarray(e, a.dtype), x, neutral)

    def one(hop, state):
        return join(
            state,
            jax.tree.map(
                lambda a, own: lax.dynamic_index_in_dim(a, hop, 0, False).astype(own.dtype),
                gathered,
                x,
            ),
        )

    return lax.fori_loop(0, place, one, state)


def join_states(earlier, later):
    decay_early, state_early = earlier
    decay_late, state_late = later
    return (decay_early * decay_late, decay_late[..., None] * state_early + state_late)


def mixer_half(
    query_logits,
    forget_gate_logits,
    written_values,
    output_gate_logits,
    gap,
    extra_log_forget,
    head_norm_scale,
    mixer_output_matrix,
):
    tokens, channels = query_logits.shape
    local_heads = channels // HEAD_DIM
    final_result = gap * jax.nn.sigmoid(-forget_gate_logits.astype(jnp.float32))
    decay_logarithm = jnp.log1p(-final_result) + extra_log_forget
    queries = jax.nn.silu(query_logits.astype(jnp.float32))
    values = written_values.astype(jnp.float32)

    def by_head(array):
        return array.reshape(tokens, local_heads, HEAD_DIM).transpose(1, 0, 2)

    final_result, decay_logarithm, queries, values = (
        by_head(final_result),
        by_head(decay_logarithm),
        by_head(queries),
        by_head(values),
    )
    running = jnp.cumsum(decay_logarithm, axis=1)
    query_decayed = queries * jnp.exp(running)
    key_decayed = final_result * jnp.exp(-running)
    scores = jnp.einsum("htd,hsd->hts", query_decayed, key_decayed, precision=exact_precision)
    causal = jnp.arange(tokens)[:, None] >= jnp.arange(tokens)[None, :]
    scores = jnp.where(causal[None], scores, 0.0)
    within = jnp.einsum("hts,hsv->htv", scores, values, precision=exact_precision)
    ending = running[:, -1:, :]
    key_state = final_result * jnp.exp(ending - running)
    end_state = jnp.einsum("htd,htv->hdv", key_state, values, precision=exact_precision)
    span_decay = jnp.exp(ending[:, 0, :])
    identity = (jnp.ones_like(span_decay), jnp.zeros_like(end_state))
    _, incoming = entering((span_decay, end_state), "ep", join_states, identity)
    carried = jnp.einsum("htd,hdv->htv", query_decayed, incoming, precision=exact_precision)
    recurrent = within + carried
    scaled = recurrent * lax.rsqrt(jnp.mean(recurrent * recurrent, axis=-1, keepdims=True) + 1e-06)
    scaled = scaled.transpose(1, 0, 2).reshape(tokens, channels)
    hidden = (
        scaled * head_norm_scale * jax.nn.silu(output_gate_logits.astype(jnp.float32))
    ).astype(jnp.bfloat16)
    return lax.psum_scatter(
        jnp.dot(hidden, mixer_output_matrix, preferred_element_type=jnp.float32).astype(
            jnp.bfloat16
        ),
        "tp",
        scatter_dimension=0,
        tiled=True,
    )


def expert_half(
    expert_input_tokens,
    expert_norm_scale,
    routes,
    router_scores_chosen,
    expert_gate_matrix,
    expert_up_matrix,
    expert_down_matrix,
):
    tokens, channels = expert_input_tokens.shape
    experts = lax.axis_size("ep")
    capacity = 3 * tokens // experts
    inputs32 = expert_input_tokens.astype(jnp.float32)
    centred = inputs32 - jnp.mean(inputs32, axis=-1, keepdims=True)
    variance = jnp.mean(centred * centred, axis=-1, keepdims=True)
    normed = (centred * lax.rsqrt(variance + 1e-05) * expert_norm_scale).astype(jnp.bfloat16)
    first_weight = jax.nn.sigmoid(router_scores_chosen[:, 0] - router_scores_chosen[:, 1])
    route_weight = jnp.stack([first_weight, 1.0 - first_weight], axis=1)
    flat_routes = routes.reshape(-1)
    onehot = (flat_routes[:, None] == jnp.arange(experts, dtype=jnp.int32)[None, :]).astype(
        jnp.int32
    )
    earlier = jnp.cumsum(onehot, axis=0) - onehot
    position = jnp.sum(earlier * onehot, axis=1)
    target = flat_routes * capacity + position
    token_ids = jnp.arange(2 * tokens, dtype=jnp.int32) // 2
    owner = jnp.zeros((experts * capacity,), jnp.int32).at[target].set(token_ids)
    filled = jnp.zeros((experts * capacity,), jnp.bool_).at[target].set(True)
    local_gate = expert_gate_matrix[0]
    local_up = expert_up_matrix[0]
    local_down = expert_down_matrix[0]
    slice_width = channels // lax.axis_size("tp")
    own_columns = lax.dynamic_slice_in_dim(
        normed, lax.axis_index("tp") * slice_width, slice_width, 1
    )
    outgoing = jnp.where(filled[:, None], own_columns[owner], jnp.zeros((), jnp.bfloat16))
    arrived = lax.all_to_all(outgoing, "ep", split_axis=0, concat_axis=0, tiled=True)
    features = lax.all_gather(arrived, "tp", axis=1, tiled=True)
    gate_act = jnp.dot(features, local_gate, preferred_element_type=jnp.float32)
    up_act = jnp.dot(features, local_up, preferred_element_type=jnp.float32)
    hidden = (jax.nn.silu(gate_act) * up_act).astype(jnp.bfloat16)
    summed = lax.psum_scatter(
        lax.dot_general(
            local_down, hidden, (((1,), (1,)), ((), ())), preferred_element_type=jnp.float32
        ).astype(jnp.bfloat16),
        "tp",
        scatter_dimension=0,
        tiled=True,
    )
    returned = lax.all_to_all(summed, "ep", split_axis=1, concat_axis=1, tiled=True)
    chosen = returned.T[target].astype(jnp.float32).reshape(tokens, 2, -1)
    return jnp.sum(chosen * route_weight[:, :, None], axis=1).astype(jnp.bfloat16)


def body(
    query_logits,
    forget_gate_logits,
    written_values,
    output_gate_logits,
    gap,
    extra_log_forget,
    head_norm_scale,
    mixer_output_matrix,
    expert_input_tokens,
    expert_norm_scale,
    routes,
    router_scores_chosen,
    expert_gate_matrix,
    expert_up_matrix,
    expert_down_matrix,
):
    mixer_output_rows = mixer_half(
        query_logits,
        forget_gate_logits,
        written_values,
        output_gate_logits,
        gap,
        extra_log_forget,
        head_norm_scale,
        mixer_output_matrix,
    )
    expert_out = expert_half(
        expert_input_tokens,
        expert_norm_scale,
        routes,
        router_scores_chosen,
        expert_gate_matrix,
        expert_up_matrix,
        expert_down_matrix,
    )
    return (mixer_output_rows, expert_out)


def solution(mesh):
    return jax.shard_map(
        body,
        mesh=mesh,
        in_specs=(
            P("ep", "tp"),
            P("ep", "tp"),
            P("ep", "tp"),
            P("ep", "tp"),
            P("tp"),
            P("ep", "tp"),
            P("tp"),
            P("tp", None),
            P("ep", None),
            P(),
            P("ep", None),
            P("ep", None),
            P("ep", None, "tp"),
            P("ep", None, "tp"),
            P("ep", None, "tp"),
        ),
        out_specs=(P(("ep", "tp"), None), P("ep", "tp")),
        check_vma=False,
    )
```

profile of v0, /device:TPU:0, one launch (start us, length us, event | category | flops | bytes accessed | tf_op | source)
XLA Modules:
  0.0 200.6 jit_solution(9134592011714128732)
XLA Ops:
  9.2 1.4 convert_reduce_fusion
  10.6 2.9 %multiply_reduce_fusion = (f32[256]{0:T(256)S(1)}, f32[256,2048]{1,0:T(8,128)}) fusion(f32[256]{0:T(256)S(1)} %broadcast_multiply_fusion.1, bf16[256,2048]{1,0:T(8,128)(2,1)} %param.25), kind=kLoop, calls=%fused_computation.18 | loop fusion | flops 2096896 | bytes 3147776 | tf_op jit(solution)/shard_map/reduce_sum | solution.py:108
  15.3 2.4 %scatter_custom_fusion.1 = s32[768]{0:T(1024)S(1)} fusion(s32[512]{0:T(512)S(1)} %bitcast.121, s32[512]{0:T(512)S(1)} %add_select_fusion, s32[]{:T(128)} %constant.71.clone.1), kind=kCustom, calls=%fused_computation.80 | custom fusion | bytes 3076 | tf_op jit(solution)/shard_map/scatter | solution.py:120
  17.8 2.4 %scatter_custom_fusion = pred[768]{0:T(1024)(128)(4,1)S(1)} fusion(s32[512]{0:T(512)S(1)} %bitcast.122, pred[512]{0:T(512)(128)(4,1)S(1)} %broadcast.132, pred[]{:T(512)} %constant.76.clone.1), kind=kCustom, calls=%fused_computation.84 | custom fusion | bytes 769 | tf_op jit(solution)/shard_map/scatter | solution.py:121
  22.3 2.7 %gather_fusion = bf16[768,512]{1,0:T(8,128)(2,1)S(1)} fusion(bf16[256,512]{1,0:T(8,128)(2,1)S(1)} %fusion.22, s32[1024]{0:T(1024)S(1)} %pad_clamp_fusion.1), kind=kCustom, calls=%fused_computation | custom fusion | bytes 1575936 | tf_op jit(solution)/shard_map/gather | solution.py:129
  25.2 27.3 %all_to_all.21 = bf16[8,96,512]{2,1,0:T(8,128)(2,1)} all-to-all(bf16[8,96,512]{2,1,0:T(8,128)(2,1)S(1)} %broadcast_select_fusion), channel_id=1, replica_groups=mesh['ep'=8,'tp'=4] {'ep'}, dimensions={0} | all-to-all | bytes 1572864 | tf_op jit(solution)/shard_map/all_to_all | solution.py:130
  58.1 2.1 %copy.99 = f32[256,4,128]{2,1,0:T(4,128)} copy(f32[256,4,128]{0,2,1:T(8,128)} %bitcast.115) | data formatting | bytes 1048576 | tf_op jit(solution)/shard_map/reshape | solution.py:56
  60.3 1.8 copy.91
  64.9 2.7 %bitcast_multiply_fusion.3 = (f32[4,256,128]{2,0,1:T(4,128)}, f32[4,256,128]{2,0,1:T(4,128)S(1)}, f32[4,256,128]{2,0,1:T(4,128)S(1)}) fusion(f32[256,4,128]{2,1,0:T(4,128)} %copy.99, f32[4,128,256]{1,2,0:T(8,128)S(1)} %bitcast.110, f32[4,128]{1,0:T(4,128)S(1)} %get-tuple-element.64, f32[256,4,128]{2,1,0:T(4,128)} %copy.92), kind=kLoop, calls=%fused_computation.41 | loop fusion | flops 655360 | bytes 3147776 | tf_op jit(solution)/shard_map/mul | solution.py:66
  69.1 11.1 %all-gather.5.cloned.1.call-done = bf16[768,2048]{1,0:T(8,128)(2,1)} async-done(((bf16[768,512]{1,0:T(8,128)(2,1)}), bf16[768,2048]{1,0:T(8,128)(2,1)}) %all-gather.5.cloned.1.call-update) | async-done | bytes 3145744 | tf_op jit(solution)/shard_map/all_gather | solution.py:131
  80.2 6.3 %fusion.2 = f32[768,1024]{1,0:T(8,128)S(1)} fusion(bf16[768,2048]{1,0:T(8,128)(2,1)} %all-gather.5.cloned.1.call-done, bf16[1,2048,1024]{2,1,0:T(8,128)(2,1)} %param.30), kind=kOutput, calls=%fused_computation.8 | convolution fusion | flops 3221225472 | bytes 10485760 | tf_op jit(solution)/shard_map/dot_general | solution.py:133
  86.6 3.8 %multiply_convert_fusion = bf16[768,1024]{1,0:T(8,128)(2,1)S(1)} fusion(f32[768,1024]{1,0:T(8,128)S(1)} %fusion.2, bf16[768,2048]{1,0:T(8,128)(2,1)S(1)} %copy-done.9, bf16[1,2048,1024]{2,1,0:T(8,128)(2,1)S(1)} %copy-done.7), kind=kOutput, calls=%fused_computation.13 | convolution fusion | flops 3225944064 | bytes 12058624 | tf_op jit(solution)/shard_map/dot_general | solution.py:132
  90.4 4.9 %fusion.9 = bf16[2048,768]{0,1:T(8,128)(2,1)} fusion(bf16[768,1024]{1,0:T(8,128)(2,1)S(1)} %multiply_convert_fusion, bf16[1,2048,1024]{2,1,0:T(8,128)(2,1)S(1)} %copy-done.8), kind=kOutput, calls=%fused_computation.14 | convolution fusion | flops 3222798336 | bytes 8912896 | tf_op jit(solution)/shard_map/dot_general | solution.py:136
  95.4 26.8 %all-gather = bf16[32,1,128]{2,1,0:T(2,128)(2,1)S(1)} all-gather(bf16[4,1,128]{2,1,0:T(2,128)(2,1)S(1)} %copy.104), channel_id=2, replica_groups=mesh['ep'=8,'tp'=4] {'ep'}, dimensions={0}, use_global_device_ids=true | all-gather | bytes 9216 | tf_op jit(solution)/shard_map/all_gather | solution.py:15
  122.2 1.8 copy.108
  124.0 2.0 convolution_select_fusion
  126.7 2.0 multiply_reduce_fusion.2
  129.0 1.7 convolution_convert_fusion
  130.7 31.4 %reduce-scatter.5.cloned.1.call-done = bf16[512,768]{0,1:T(8,128)(2,1)} async-done(((bf16[2048,768]{0,1:T(8,128)(2,1)}), bf16[512,768]{0,1:T(8,128)(2,1)}) %reduce-scatter.5.cloned.1.call-update) | async-done | bytes 786448 | tf_op jit(solution)/shard_map/reduce_scatter | solution.py:135
  162.1 5.5 %all-to-all-start.1 = ((bf16[512,8,96]{0,2,1:T(8,128)(2,1)}), bf16[512,8,96]{0,2,1:T(8,128)(2,1)S(1)}, u32[]{:S(2)}, u32[]{:S(2)}) async-start(bf16[512,8,96]{0,2,1:T(8,128)(2,1)} %bitcast.117), calls=%async_computation.3 | async-start | bytes 1572864 | tf_op jit(solution)/shard_map/all_to_all | solution.py:143
  167.8 19.9 %all-to-all-done.1 = bf16[512,8,96]{0,2,1:T(8,128)(2,1)S(1)} async-done(((bf16[512,8,96]{0,2,1:T(8,128)(2,1)}), bf16[512,8,96]{0,2,1:T(8,128)(2,1)S(1)}, u32[]{:S(2)}, u32[]{:S(2)}) %all-to-all-start.1) | async-done | bytes 786464 | tf_op jit(solution)/shard_map/all_to_all | solution.py:143
  187.7 2.6 %gather_fusion.1 = bf16[512,512]{1,0:T(8,128)(2,1)} fusion(bf16[768,512]{1,0:T(8,128)(2,1)S(1)} %bitcast.108, s32[1024]{0:T(1024)S(1)} %pad_clamp_fusion), kind=kCustom, calls=%fused_computation.1 | custom fusion | bytes 1050624 | tf_op jit(solution)/shard_map/gather | solution.py:144
  190.3 1.7 reshape.160
  192.0 2.1 %multiply_reduce_fusion.1 = bf16[256,512]{1,0:T(8,128)(2,1)} fusion(f32[256,2,512]{2,1,0:T(2,128)S(1)} %reshape.160, f32[256,2]{1,0:T(8,128)S(1)} %copy.112), kind=kLoop, calls=%fused_computation.22 | loop fusion | flops 393216 | bytes 1312768 | tf_op jit(solution)/shard_map/reduce_sum | solution.py:145
  (81 shorter events, 17.1 us)
Async XLA Ops:
  7.2 121.8 %copy-start = (bf16[512,2048]{1,0:T(8,128)(2,1)S(1)}, bf16[512,2048]{1,0:T(8,128)(2,1)}, u32[]{:S(2)}) copy-start(bf16[512,2048]{1,0:T(8,128)(2,1)} %param.24) | copy-start | bytes 6291460
  7.2 73.0 %all-gather.5.cloned.1.call-start = ((), (), s32[]{:S(2)}) async-start(), calls=%async_computation.5 | async-start | bytes 3932160 | tf_op jit(solution)/shard_map/all_gather | solution.py:131
  25.0 29.9 %copy-start.6 = (f32[512]{0:T(512)S(1)}, f32[512]{0:T(512)}, u32[]{:S(2)}) copy-start(f32[512]{0:T(512)} %param.21) | copy-start | bytes 6148
  52.5 73.5 %all-gather.7.cloned.1.call-start = ((), (), s32[]{:S(2)}) async-start(), calls=%async_computation.7 | async-start | bytes 1179648 | tf_op jit(solution)/shard_map/all_gather | solution.py:15
  58.1 9.5 %copy-start.2 = (bf16[256,512]{1,0:T(8,128)(2,1)S(1)}, bf16[256,512]{1,0:T(8,128)(2,1)}, u32[]{:S(2)}) copy-start(bf16[256,512]{1,0:T(8,128)(2,1)} %param.19) | copy-start | bytes 786436
  68.9 93.2 %reduce-scatter.5.cloned.1.call-start = ((), (), s32[]{:S(2)}) async-start(), calls=%async_computation.6 | async-start | bytes 3932160 | tf_op jit(solution)/shard_map/reduce_scatter | solution.py:135
  80.2 6.3 %copy-start.7 = (bf16[1,2048,1024]{2,1,0:T(8,128)(2,1)S(1)}, bf16[1,2048,1024]{2,1,0:T(8,128)(2,1)}, u32[]{:S(2)}) copy-start(bf16[1,2048,1024]{2,1,0:T(8,128)(2,1)} %param.29) | copy-start | bytes 12582916
  80.2 6.3 %copy-start.9 = (bf16[768,2048]{1,0:T(8,128)(2,1)S(1)}, bf16[768,2048]{1,0:T(8,128)(2,1)}, u32[]{:S(2)}) copy-start(bf16[768,2048]{1,0:T(8,128)(2,1)} %all-gather.5.cloned.1.call-done) | copy-start | bytes 9437188
  86.5 3.8 %copy-start.8 = (bf16[1,2048,1024]{2,1,0:T(8,128)(2,1)S(1)}, bf16[1,2048,1024]{2,1,0:T(8,128)(2,1)}, u32[]{:S(2)}) copy-start(bf16[1,2048,1024]{2,1,0:T(8,128)(2,1)} %param.31) | copy-start | bytes 12582916
  95.3 28.7 %copy-start.1 = (f32[4,256,128]{2,0,1:T(4,128)S(1)}, f32[4,256,128]{2,0,1:T(4,128)}, u32[]{:S(2)}) copy-start(f32[4,256,128]{2,0,1:T(4,128)} %get-tuple-element.61) | copy-start | bytes 1572868
  95.3 98.8 %reduce-scatter.3.cloned.1.call-start = ((), (), s32[]{:S(2)}) async-start(), calls=%async_computation.4 | async-start | bytes 1310720 | tf_op jit(solution)/shard_map/reduce_scatter | solution.py:84
  126.1 2.7 %copy-start.3 = (bf16[256,512]{0,1:T(8,128)(2,1)S(1)}, bf16[256,512]{0,1:T(8,128)(2,1)}, u32[]{:S(2)}) copy-start(bf16[256,512]{0,1:T(8,128)(2,1)} %copy.108) | copy-start | bytes 786436
  126.1 2.7 %copy-start.4 = (f32[512]{0:T(512)S(1)}, f32[512]{0:T(512)}, u32[]{:S(2)}) copy-start(f32[512]{0:T(512)} %param.23) | copy-start | bytes 6148
  129.0 38.7 %copy-start.5 = (f32[256,2]{0,1:T(2,128)S(1)}, f32[256,2]{0,1:T(2,128)}, u32[]{:S(2)}) copy-start(f32[256,2]{0,1:T(2,128)} %param.28) | copy-start | bytes 6148
  162.1 25.6 %all-to-all-start.1 = ((bf16[512,8,96]{0,2,1:T(8,128)(2,1)}), bf16[512,8,96]{0,2,1:T(8,128)(2,1)S(1)}, u32[]{:S(2)}, u32[]{:S(2)}) async-start(bf16[512,8,96]{0,2,1:T(8,128)(2,1)} %bitcast.117), calls=%async_computation.3 | async-start | bytes 1572864 | tf_op jit(solution)/shard_map/all_to_all | solution.py:143
Sparse Core Ops, SparseCore 0:
  52.6 27.5 all-gather.4
  82.9 40.3 all-gather.6
  125.8 36.2 reduce-scatter.4
  165.1 24.7 reduce-scatter.2
where the time goes:
time: 201 us
  waiting for transfers between devices  62.5 us (31%)
  blocking collectives  54.2 us (27%)
  local copies, waits for them, and re-layouts  25.1 us (12%)
  matrix products  22.6 us (11%)
  other arithmetic  16.3 us (8%)
  between operations  14.1 us (7%)
  starting transfers between devices  5.85 us (3%)
    reduce_scatter x1, waiting for transfers between devices, expert_half(): lax.psum_scatter(lax.dot_general(local_down, hidden, (((1,), (1,)), ((),...  31.4 us
    all_to_all x1, blocking collectives, expert_half(): lax.all_to_all(outgoing, 'ep', split_axis=0, concat_axis=0, tiled=True)  27.3 us
    all_gather x1, blocking collectives, entering(): lax.all_gather(a.astype(kind), axis)  26.8 us
    all_to_all x1, waiting for transfers between devices, expert_half(): lax.all_to_all(summed, 'ep', split_axis=1, concat_axis=1, tiled=True)  19.9 us
    all_gather x1, waiting for transfers between devices, expert_half(): features = lax.all_gather(arrived, 'tp', axis=1, tiled=True)  11.1 us
    unnamed x26, local copies, waits for them, and re-layouts  6.94 us
    dot_general x1, matrix products, expert_half(): up_act = jnp.dot(features, local_up, preferred_element_type=jnp.float32)  6.28 us
    all_to_all x1, starting transfers between devices, expert_half(): lax.all_to_all(summed, 'ep', split_axis=1, concat_axis=1, tiled=True)  5.51 us
  transfers between devices with their start and end apart: 5, of which 3 were waited for; matrix products, arithmetic and copies ran while one was open for 23% of the time, Pallas kernels for 0%

commit v1 on v0

v1 whole, which is shorter than its diff:
```python
import functools

import jax
import jax.numpy as jnp
from jax import lax
from jax.experimental import pallas as pl
from jax.experimental.pallas import tpu as pltpu
from jax.sharding import PartitionSpec as P

HEAD_DIM = 128
SPAN = 128
CHUNKS = 1
f32, bf16 = jnp.float32, jnp.bfloat16
NT = (((1,), (1,)), ((), ()))
TN = (((0,), (0,)), ((), ()))


def dot(a, b, dims=(((1,), (0,)), ((), ())), precision=None):
    return lax.dot_general(a, b, dims, precision=precision, preferred_element_type=f32)


def sigmoid(v):
    return 1.0 / (1.0 + jnp.exp(-v))


def mixer_local(q_ref, f_ref, v_ref, extra_ref, gap_ref, within_ref, qdec_ref, packed_ref):
    tokens, channels = q_ref.shape
    row = lax.broadcasted_iota(jnp.int32, (SPAN, SPAN), 0)
    col = lax.broadcasted_iota(jnp.int32, (SPAN, SPAN), 1)
    causal = row >= col
    lower = causal.astype(f32)
    heads = channels // HEAD_DIM
    state = [None] * heads
    total_before = jnp.zeros((1, channels), f32)
    for c in range(tokens // SPAN):
        rows = slice(c * SPAN, (c + 1) * SPAN)
        key = gap_ref[...] * sigmoid(-f_ref[rows, :].astype(f32))
        decay = jnp.log1p(-key) + extra_ref[rows, :]
        run = dot(lower, decay, precision=lax.Precision.HIGHEST)
        middle, total = run[SPAN // 2 - 1 : SPAN // 2, :], run[SPAN - 1 :, :]
        q32 = q_ref[rows, :].astype(f32)
        query = q32 * sigmoid(q32)
        q_mid = (query * jnp.exp(run - middle)).astype(bf16)
        k_mid = (key * jnp.exp(middle - run)).astype(bf16)
        q_run = query * jnp.exp(run)
        k_end = (key * jnp.exp(total - run)).astype(bf16)
        qdec_ref[rows, :] = (q_run * jnp.exp(total_before)).astype(bf16)
        q_run = q_run.astype(bf16)
        gone = jnp.exp(total)
        values = v_ref[rows, :]
        for h in range(heads):
            lanes = slice(h * HEAD_DIM, (h + 1) * HEAD_DIM)
            vh = values[:, lanes]
            scores = jnp.where(causal, dot(q_mid[:, lanes], k_mid[:, lanes], NT), 0.0)
            within = dot(scores.astype(bf16), vh)
            added = dot(vh, k_end[:, lanes], TN)
            if c:
                within = within + dot(q_run[:, lanes], state[h].astype(bf16), NT)
                state[h] = state[h] * gone[:, lanes] + added
            else:
                state[h] = added
            within_ref[rows, lanes] = within
        total_before = total_before + total
    span_decay = jnp.exp(total_before)
    extra_rows = packed_ref.shape[1] - HEAD_DIM
    for h in range(heads):
        lanes = slice(h * HEAD_DIM, (h + 1) * HEAD_DIM)
        packed_ref[h, :HEAD_DIM, :] = state[h]
        packed_ref[h, HEAD_DIM:, :] = jnp.broadcast_to(span_decay[:, lanes], (extra_rows, HEAD_DIM))


def mixer_finish(within_ref, qdec_ref, incoming_ref, gate_ref, scale_ref, w_ref, out_ref):
    channels = within_ref.shape[1]
    pieces = []
    for h in range(channels // HEAD_DIM):
        lanes = slice(h * HEAD_DIM, (h + 1) * HEAD_DIM)
        rec = within_ref[:, lanes] + dot(
            qdec_ref[:, lanes], incoming_ref[h, :HEAD_DIM, :].astype(bf16), NT
        )
        norm = lax.rsqrt(jnp.mean(rec * rec, axis=-1, keepdims=True) + 1e-06)
        gate = gate_ref[:, lanes].astype(f32)
        pieces.append((rec * norm * scale_ref[:, lanes] * (gate * sigmoid(gate))).astype(bf16))
    out_ref[...] = dot(jnp.concatenate(pieces, axis=1), w_ref[...]).astype(bf16)


def shifted(step, x):
    size = lax.axis_size("ep")
    links = [(i, i + step) for i in range(size - step)]
    early = lax.ppermute(x.astype(bf16), "ep", links).astype(f32)
    is_state = jnp.arange(x.shape[1])[None, :, None] < HEAD_DIM
    return jnp.where(lax.axis_index("ep") >= step, early, jnp.where(is_state, 0.0, 1.0))


def joined(step, late):
    early = shifted(step, late)
    is_state = jnp.arange(late.shape[1])[None, :, None] < HEAD_DIM
    decay = late[:, HEAD_DIM : HEAD_DIM + 1, :]
    return early * decay + jnp.where(is_state, late, 0.0)


def mixer_begin(query, forget, values, gap, extra):
    tokens, channels = query.shape
    heads = channels // HEAD_DIM
    within, qdec, packed = pl.pallas_call(
        mixer_local,
        name="mixer_local",
        out_shape=(
            jax.ShapeDtypeStruct((tokens, channels), f32),
            jax.ShapeDtypeStruct((tokens, channels), bf16),
            jax.ShapeDtypeStruct((heads, HEAD_DIM + 16, HEAD_DIM), f32),
        ),
    )(query, forget, values, extra, gap[None, :])
    return within, qdec, joined(1, shifted(1, packed))


def mixer_end(within, qdec, state, output_gate, head_scale, matrix):
    step = 2
    while step < lax.axis_size("ep") - 1:
        state = joined(step, state)
        step *= 2
    mixed = pl.pallas_call(
        mixer_finish,
        name="mixer_finish",
        out_shape=jax.ShapeDtypeStruct((within.shape[0], matrix.shape[1]), bf16),
    )(within, qdec, state, output_gate, head_scale[None, :], matrix)
    return lax.psum_scatter(mixed, "tp", scatter_dimension=0, tiled=True)


def dispatch(experts, capacity, place_ref, x_ref, own_ref, scale_ref, routes_ref, out_ref, slot_ref):
    tokens = x_ref.shape[0]
    x = x_ref[...].astype(f32)
    mean = jnp.mean(x, axis=-1, keepdims=True)
    centred = x - mean
    norm = lax.rsqrt(jnp.mean(centred * centred, axis=-1, keepdims=True) + 1e-05)
    own = ((own_ref[...].astype(f32) - mean) * norm * scale_ref[...]).astype(bf16)
    names = lax.broadcasted_iota(jnp.int32, (max(experts, 16), tokens), 0)
    first, second = routes_ref[0:1, :], routes_ref[1:2, :]
    is_first, is_second = names == first, names == second
    chosen = (is_first | is_second).astype(f32)
    before = (
        lax.broadcasted_iota(jnp.int32, (tokens, tokens), 0)
        < lax.broadcasted_iota(jnp.int32, (tokens, tokens), 1)
    ).astype(f32)
    position = dot(chosen.astype(bf16), before.astype(bf16))
    part = capacity // CHUNKS

    def slot(is_one, route):
        pos = jnp.sum(jnp.where(is_one, position, 0.0), axis=0, keepdims=True).astype(jnp.int32)
        chunk = sum((pos >= part * i).astype(jnp.int32) for i in range(1, CHUNKS))
        return (chunk * experts + route) * part + pos - chunk * part

    slot_first, slot_second = slot(is_first, first), slot(is_second, second)
    slots = lax.broadcasted_iota(jnp.int32, (out_ref.shape[0], tokens), 0)
    pick = jnp.where((slots == slot_first) | (slots == slot_second), 1.0, 0.0).astype(bf16)
    out_ref[...] = dot(pick, own).astype(bf16)
    which = lax.broadcasted_iota(jnp.int32, slot_ref.shape, 0)
    slot_ref[...] = jnp.where(which == 0, slot_first, slot_second)


def combine(slot_ref, scores_ref, *refs):
    out_ref, back = refs[-1], refs[:-1]
    first = sigmoid(scores_ref[:, 0:1] - scores_ref[:, 1:2])
    tokens = out_ref.shape[0]
    rows = back[0].shape[0]
    parts = []
    for k in range(2):
        total = None
        for c, ref in enumerate(back):
            slots = lax.broadcasted_iota(jnp.int32, (rows, tokens), 0) + c * rows
            pick = jnp.where(slots == slot_ref[k : k + 1, :], 1.0, 0.0).astype(bf16)
            term = dot(pick, ref[...], TN)
            total = term if total is None else total + term
        parts.append(total)
    out_ref[...] = (parts[0] * first + parts[1] * (1.0 - first)).astype(bf16)


def exchange(x, axis):
    return lax.all_to_all(x, axis, split_axis=0, concat_axis=0, tiled=True)


def expert_half(state, x, scale, routes, scores, gate_w, up_w, down_w):
    tokens, channels = x.shape
    experts, groups = lax.axis_size("ep"), lax.axis_size("tp")
    capacity = 3 * tokens // experts
    width = channels // groups
    total_slots = experts * capacity
    outgoing, slot = pl.pallas_call(
        functools.partial(dispatch, experts, capacity),
        name="dispatch",
        grid_spec=pltpu.PrefetchScalarGridSpec(
            num_scalar_prefetch=1,
            grid=(1,),
            in_specs=[
                pl.BlockSpec((tokens, channels), lambda i, s: (0, 0)),
                pl.BlockSpec((tokens, width), lambda i, s: (0, s[0])),
                pl.BlockSpec((1, width), lambda i, s: (0, s[0])),
                pl.BlockSpec((2, tokens), lambda i, s: (0, 0)),
            ],
            out_specs=[
                pl.BlockSpec((total_slots, width), lambda i, s: (0, 0)),
                pl.BlockSpec((8, tokens), lambda i, s: (0, 0)),
            ],
        ),
        out_shape=(
            jax.ShapeDtypeStruct((total_slots, width), bf16),
            jax.ShapeDtypeStruct((8, tokens), jnp.int32),
        ),
    )(lax.axis_index("tp").astype(jnp.int32)[None], x, x, scale[None, :], routes.T)
    rows = total_slots // CHUNKS
    back = []
    for c in range(CHUNKS):
        arrived = exchange(outgoing[c * rows : (c + 1) * rows], "ep")
        features = lax.all_gather(arrived, "tp", axis=1, tiled=True)
        features, state = lax.optimization_barrier((features, state))
        gate, up = dot(features, gate_w[0]), dot(features, up_w[0])
        hidden = (jax.nn.silu(gate) * up).astype(bf16)
        result = dot(hidden, down_w[0], NT).astype(bf16)
        summed = lax.psum_scatter(result, "tp", scatter_dimension=1, tiled=True)
        back.append(exchange(summed, "ep"))
    combined = pl.pallas_call(
        combine, name="combine", out_shape=jax.ShapeDtypeStruct((tokens, width), bf16)
    )(slot, scores, *back)
    return state, combined


def body(q, f, v, og, gap, extra, head_scale, matrix, x, scale, routes, scores, gw, uw, dw):
    within, qdec, state = mixer_begin(q, f, v, gap, extra)
    state, expert_out = expert_half(state, x, scale, routes, scores, gw, uw, dw)
    mixer_output_rows = mixer_end(within, qdec, state, og, head_scale, matrix)
    return (mixer_output_rows, expert_out)


def solution(mesh):
    wide, experts = P("ep", "tp"), P("ep", None, "tp")
    rows = P("ep", None)
    mixer_specs = (wide, wide, wide, wide, P("tp"), wide, P("tp"), P("tp", None))
    expert_specs = (rows, P(), rows, rows, experts, experts, experts)
    return jax.shard_map(
        body,
        mesh=mesh,
        in_specs=mixer_specs + expert_specs,
        out_specs=(P(("ep", "tp"), None), P("ep", "tp")),
        check_vma=False,
    )
```

time: 201 us -> 155 us (0.77)
  blocking collectives: 54.2 us -> 27.5 us
  local copies, waits for them, and re-layouts: 25.1 us -> 1.72 us
  starting transfers between devices: 5.85 us -> 22.1 us
  other arithmetic: 16.3 us -> 2.31 us
  Pallas kernels: 0 us -> 13.9 us
  matrix products: 22.6 us -> 15 us
  waiting for transfers between devices: 62.5 us -> 57.7 us
    all_gather x1 -> x0, blocking collectives: 26.8 us -> none  [entering(): lax.all_gather(a.astype(kind), axis)]
    ppermute x0 -> x4, starting transfers between devices: none -> 16.4 us  [shifted(): early = lax.ppermute(x.astype(bf16), 'ep', links).astype(f32)]
    pallas_call x0 -> x4, Pallas kernels: none -> 13.9 us  [the longest x1 4.39 us: mixer_end(): pl.pallas_call(mixer_finish, name='mixer_finish', out_shape=jax.ShapeDtyp...]
    reduce_scatter x2, waiting for transfers between devices: 31.4 us -> 17.5 us  [the longest x1 17.5 us: expert_half(): summed = lax.psum_scatter(result, 'tp', scatter_dimension=1, tiled=True)]
    ppermute x0 -> x4, waiting for transfers between devices: none -> 11.3 us  [shifted(): early = lax.ppermute(x.astype(bf16), 'ep', links).astype(f32)]
    dot_general x8 -> x3, matrix products: 22.6 us -> 15 us  [dot(): lax.dot_general(a, b, dims, precision=precision, preferred_element_type=f32)]
    reduce_sum x4 -> x0, other arithmetic: 6.49 us -> none  [the longest x1 2.91 us: expert_half(): variance = jnp.mean(centred * centred, axis=-1, keepdims=True)]
    mul x5 -> x0, other arithmetic: 5.66 us -> none  [the longest x1 2.69 us: mixer_half(): key_decayed = final_result * jnp.exp(-running)]
  transfers between devices with their start and end apart: 5 -> 8, of which waited for: 3 -> 7; matrix products, arithmetic and copies ran while one was open for 23% -> 2% of each run, Pallas kernels for 0% -> 7%
where the time goes in v1:
time: 155 us; the launch traced here: 154 us
  waiting for transfers between devices  57.7 us (37%)
  blocking collectives  27.5 us (18%)
  starting transfers between devices  22.1 us (14%)
  matrix products  15 us (10%)
  Pallas kernels  13.9 us (9%)
  between operations  13.9 us (9%)
  other arithmetic  2.31 us (1%)
  local copies, waits for them, and re-layouts  1.72 us (1%)
    all_to_all x1, blocking collectives, exchange(): return lax.all_to_all(x, axis, split_axis=0, concat_axis=0, tiled=True)  27.5 us
    all_to_all x1, waiting for transfers between devices, exchange(): return lax.all_to_all(x, axis, split_axis=0, concat_axis=0, tiled=True)  19.3 us
    reduce_scatter x1, waiting for transfers between devices, expert_half(): summed = lax.psum_scatter(result, 'tp', scatter_dimension=1, tiled=True)  17.5 us
    ppermute x4, starting transfers between devices, shifted(): early = lax.ppermute(x.astype(bf16), 'ep', links).astype(f32)  16.4 us
    dot_general x3, matrix products, dot(): lax.dot_general(a, b, dims, precision=precision, preferred_element_type=f32)  15 us
    ppermute x4, waiting for transfers between devices, shifted(): early = lax.ppermute(x.astype(bf16), 'ep', links).astype(f32)  11.3 us
    all_gather x1, waiting for transfers between devices, expert_half(): features = lax.all_gather(arrived, 'tp', axis=1, tiled=True)  9.61 us
    all_to_all x1, starting transfers between devices, exchange(): return lax.all_to_all(x, axis, split_axis=0, concat_axis=0, tiled=True)  5.5 us
  transfers between devices with their start and end apart: 8, of which 7 were waited for; matrix products, arithmetic and copies ran while one was open for 2% of the time, Pallas kernels for 7%

profile of v1, /device:TPU:0, one launch (start us, length us, event | category | flops | bytes accessed | tf_op | source)
XLA Modules:
  0.0 154.2 jit_solution(8913027291246610212)
XLA Ops:
  7.2 3.2 %dispatch.1 = (bf16[768,512]{1,0:T(8,128)(2,1)}, s32[8,256]{1,0:T(8,128)}) custom-call(s32[1]{0:T(128)} %bitcast.1.place_ref, bf16[256,2048]{1,0:T(8,128)(2,1)} %own_ref.1, bf16[256,2048]{1,0:T(8,128)(2,1)} %own_ref.1, f32[1,2048]{1,0:T(1,128)} %bitcast.32, s32[2,256]{1,0:T(2,128)} %bitcast.38), custom_call_target="tpu_custom_call" | custom-call | tf_op jit(solution)/shard_map/dispatch/pallas_call | solution.py:187
  10.4 27.5 %all_to_all.23 = bf16[8,96,512]{2,1,0:T(8,128)(2,1)} all-to-all(bf16[8,96,512]{2,1,0:T(8,128)(2,1)} %bitcast.31), channel_id=1, replica_groups=mesh['ep'=8,'tp'=4] {'ep'}, dimensions={0} | all-to-all | bytes 1572864 | tf_op jit(solution)/shard_map/all_to_all | solution.py:178
  38.0 3.8 %mixer_local.1 = (f32[256,512]{1,0:T(8,128)}, bf16[256,512]{1,0:T(8,128)(2,1)}, f32[4,144,128]{2,1,0:T(8,128)}) custom-call(bf16[256,512]{1,0:T(8,128)(2,1)} %q_ref.1, bf16[256,512]{1,0:T(8,128)(2,1)} %f_ref.1, bf16[256,512]{1,0:T(8,128)(2,1)} %v_ref.1, f32[256,512]{1,0:T(8,128)} %extra_ref.1, f32[1,512]{1,0:T(1,128)} %bitcast.36), custom_call_target="tpu_custom_call" | custom-call | tf_op jit(solution)/shard_map/mixer_local/pallas_call | solution.py:104
  41.8 1.0 convert_element_type.30
  42.8 3.3 %collective-permute-start = (bf16[4,144,128]{2,1,0:T(8,128)(2,1)S(1)}, bf16[4,144,128]{2,1,0:T(8,128)(2,1)S(1)}, u32[]{:S(2)}, u32[]{:S(2)}) collective-permute-start(bf16[4,144,128]{2,1,0:T(8,128)(2,1)S(1)} %convert_element_type.30), channel_id=1, source_target_pairs={{0,4},{4,8},{8,12},{12,16},{16,20},{20,24},{24,28},{1,5},{5,9},{9,... | collective-permute-start | bytes 442376 | tf_op jit(solution)/shard_map/ppermute | solution.py:89
  46.1 2.6 %collective-permute-done = bf16[4,144,128]{2,1,0:T(8,128)(2,1)S(1)} collective-permute-done((bf16[4,144,128]{2,1,0:T(8,128)(2,1)S(1)}, bf16[4,144,128]{2,1,0:T(8,128)(2,1)S(1)}, u32[]{:S(2)}, u32[]{:S(2)}) %collective-permute-start) | collective-permute-done | bytes 147488 | tf_op jit(solution)/shard_map/ppermute | solution.py:89
  48.9 4.4 %collective-permute-start.1 = (bf16[4,144,128]{2,1,0:T(8,128)(2,1)S(1)}, bf16[4,144,128]{2,1,0:T(8,128)(2,1)S(1)}, u32[]{:S(2)}, u32[]{:S(2)}) collective-permute-start(bf16[4,144,128]{2,1,0:T(8,128)(2,1)S(1)} %fusion.11), channel_id=1, source_target_pairs={{0,4},{4,8},{8,12},{12,16},{16,20},{20,24},{24,28},{1,5},{5,9},{9,... | collective-permute-start | bytes 442376 | tf_op jit(solution)/shard_map/ppermute | solution.py:89
  53.4 2.5 %collective-permute-done.1 = bf16[4,144,128]{2,1,0:T(8,128)(2,1)S(1)} collective-permute-done((bf16[4,144,128]{2,1,0:T(8,128)(2,1)S(1)}, bf16[4,144,128]{2,1,0:T(8,128)(2,1)S(1)}, u32[]{:S(2)}, u32[]{:S(2)}) %collective-permute-start.1) | collective-permute-done | bytes 147488 | tf_op jit(solution)/shard_map/ppermute | solution.py:89
  56.1 9.6 %all-gather.2.cloned.1.call-done = bf16[768,2048]{1,0:T(8,128)(2,1)} async-done(((bf16[768,512]{1,0:T(8,128)(2,1)}), bf16[768,2048]{1,0:T(8,128)(2,1)}) %all-gather.2.cloned.1.call-update) | async-done | bytes 3145744 | tf_op jit(solution)/shard_map/all_gather | solution.py:213
  65.7 6.3 %fusion.2 = f32[768,1024]{1,0:T(8,128)S(1)} fusion(bf16[768,2048]{1,0:T(8,128)(2,1)} %all-gather.2.cloned.1.call-done, bf16[1,2048,1024]{2,1,0:T(8,128)(2,1)} %param.28), kind=kOutput, calls=%fused_computation.2 | convolution fusion | flops 3221225472 | bytes 10485760 | tf_op jit(solution)/shard_map/dot_general | solution.py:19
  72.0 3.8 %multiply_convert_fusion = bf16[768,1024]{1,0:T(8,128)(2,1)S(1)} fusion(f32[768,1024]{1,0:T(8,128)S(1)} %fusion.2, bf16[768,2048]{1,0:T(8,128)(2,1)S(1)} %copy-done.4, bf16[1,2048,1024]{2,1,0:T(8,128)(2,1)S(1)} %copy-done.2), kind=kOutput, calls=%fused_computation.7 | convolution fusion | flops 3225944064 | bytes 12058624 | tf_op jit(solution)/shard_map/dot_general | solution.py:19
  75.8 4.9 %fusion.6 = bf16[768,2048]{1,0:T(8,128)(2,1)} fusion(bf16[768,1024]{1,0:T(8,128)(2,1)S(1)} %multiply_convert_fusion, bf16[1,2048,1024]{2,1,0:T(8,128)(2,1)S(1)} %copy-done.3), kind=kOutput, calls=%fused_computation.6 | convolution fusion | flops 3222798336 | bytes 8912896 | tf_op jit(solution)/shard_map/dot_general | solution.py:19
  80.8 3.4 %collective-permute-start.2 = (bf16[4,144,128]{2,1,0:T(8,128)(2,1)S(1)}, bf16[4,144,128]{2,1,0:T(8,128)(2,1)S(1)}, u32[]{:S(2)}, u32[]{:S(2)}) collective-permute-start(bf16[4,144,128]{2,1,0:T(8,128)(2,1)S(1)} %convert_element_type.34), channel_id=1, source_target_pairs={{0,8},{4,12},{8,16},{12,20},{16,24},{20,28},{1,9},{5,13},{9,17},{1... | collective-permute-start | bytes 442376 | tf_op jit(solution)/shard_map/ppermute | solution.py:89
  84.3 3.4 %collective-permute-done.2 = bf16[4,144,128]{2,1,0:T(8,128)(2,1)S(1)} collective-permute-done((bf16[4,144,128]{2,1,0:T(8,128)(2,1)S(1)}, bf16[4,144,128]{2,1,0:T(8,128)(2,1)S(1)}, u32[]{:S(2)}, u32[]{:S(2)}) %collective-permute-start.2) | collective-permute-done | bytes 147488 | tf_op jit(solution)/shard_map/ppermute | solution.py:89
  87.8 5.3 %collective-permute-start.3 = (bf16[4,144,128]{2,1,0:T(8,128)(2,1)S(1)}, bf16[4,144,128]{2,1,0:T(8,128)(2,1)S(1)}, u32[]{:S(2)}, u32[]{:S(2)}) collective-permute-start(bf16[4,144,128]{2,1,0:T(8,128)(2,1)S(1)} %get-tuple-element.16), channel_id=1, source_target_pairs={{0,16},{4,20},{8,24},{12,28},{1,17},{5,21},{9,25},{13,29},{2,18},{... | collective-permute-start | bytes 442376 | tf_op jit(solution)/shard_map/ppermute | solution.py:89
  93.2 2.7 %collective-permute-done.3 = bf16[4,144,128]{2,1,0:T(8,128)(2,1)S(1)} collective-permute-done((bf16[4,144,128]{2,1,0:T(8,128)(2,1)S(1)}, bf16[4,144,128]{2,1,0:T(8,128)(2,1)S(1)}, u32[]{:S(2)}, u32[]{:S(2)}) %collective-permute-start.3) | collective-permute-done | bytes 147488 | tf_op jit(solution)/shard_map/ppermute | solution.py:89
  95.9 0.8 select_add_fusion.incoming_ref
  96.7 4.4 %mixer_finish.1 = bf16[256,2048]{1,0:T(8,128)(2,1)} custom-call(f32[256,512]{1,0:T(8,128)} %get-tuple-element.9.within_ref, bf16[256,512]{1,0:T(8,128)(2,1)} %get-tuple-element.10.qdec_ref, f32[4,144,128]{2,1,0:T(8,128)} %select_add_fusion.incoming_ref, bf16[256,512]{1,0:T(8,128)(2,1)} %gate_ref.1, f32[1,512]{1,0:T(1,128)} %bitcast.37, bf16[512,2048]{1,0:T(8,128)(2,1)} %w_ref.1), custom_call_target="tpu_custom_call" | custom-call | tf_op jit(solution)/shard_map/mixer_finish/pallas_call | solution.py:121
  101.1 17.5 %reduce-scatter.5.cloned.1.call-done = bf16[768,512]{1,0:T(8,128)(2,1)} async-done(((bf16[768,2048]{1,0:T(8,128)(2,1)}), bf16[768,512]{1,0:T(8,128)(2,1)}) %reduce-scatter.5.cloned.1.call-update) | async-done | bytes 786448 | tf_op jit(solution)/shard_map/reduce_scatter | solution.py:218
  118.6 5.5 %all-to-all-start.1 = ((bf16[8,96,512]{2,1,0:T(8,128)(2,1)}), bf16[8,96,512]{2,1,0:T(8,128)(2,1)S(1)}, u32[]{:S(2)}, u32[]{:S(2)}) async-start(bf16[8,96,512]{2,1,0:T(8,128)(2,1)} %bitcast.30), calls=%async_computation.3 | async-start | bytes 1572864 | tf_op jit(solution)/shard_map/all_to_all | solution.py:178
  124.1 0.8 copy.17.scores_ref
  124.9 19.3 %all-to-all-done.1 = bf16[8,96,512]{2,1,0:T(8,128)(2,1)S(1)} async-done(((bf16[8,96,512]{2,1,0:T(8,128)(2,1)}), bf16[8,96,512]{2,1,0:T(8,128)(2,1)S(1)}, u32[]{:S(2)}, u32[]{:S(2)}) %all-to-all-start.1) | async-done | bytes 786464 | tf_op jit(solution)/shard_map/all_to_all | solution.py:178
  144.2 0.9 copy-done
  145.1 2.6 %combine.1 = bf16[256,512]{1,0:T(8,128)(2,1)} custom-call(s32[8,256]{1,0:T(8,128)} %get-tuple-element.14.slot_ref, f32[256,2]{1,0:T(8,128)} %copy.17.scores_ref, bf16[768,512]{1,0:T(8,128)(2,1)} %bitcast.29), custom_call_target="tpu_custom_call" | custom-call | tf_op jit(solution)/shard_map/combine/pallas_call | solution.py:220
  (26 shorter events, 0.7 us)
Async XLA Ops:
  7.2 58.5 %all-gather.2.cloned.1.call-start = ((), (), s32[]{:S(2)}) async-start(), calls=%async_computation.4 | async-start | bytes 3932160 | tf_op jit(solution)/shard_map/all_gather | solution.py:213
  38.0 80.7 %reduce-scatter.5.cloned.1.call-start = ((), (), s32[]{:S(2)}) async-start(), calls=%async_computation.6 | async-start | bytes 3932160 | tf_op jit(solution)/shard_map/reduce_scatter | solution.py:218
  42.8 6.0 %collective-permute-start = (bf16[4,144,128]{2,1,0:T(8,128)(2,1)S(1)}, bf16[4,144,128]{2,1,0:T(8,128)(2,1)S(1)}, u32[]{:S(2)}, u32[]{:S(2)}) collective-permute-start(bf16[4,144,128]{2,1,0:T(8,128)(2,1)S(1)} %convert_element_type.30), channel_id=1, source_target_pairs={{0,4},{4,8},{8,12},{12,16},{16,20},{20,24},{24,28},{1,5},{5,9},{9,... | collective-permute-start | bytes 442376 | tf_op jit(solution)/shard_map/ppermute | solution.py:89
  48.9 7.0 %collective-permute-start.1 = (bf16[4,144,128]{2,1,0:T(8,128)(2,1)S(1)}, bf16[4,144,128]{2,1,0:T(8,128)(2,1)S(1)}, u32[]{:S(2)}, u32[]{:S(2)}) collective-permute-start(bf16[4,144,128]{2,1,0:T(8,128)(2,1)S(1)} %fusion.11), channel_id=1, source_target_pairs={{0,4},{4,8},{8,12},{12,16},{16,20},{20,24},{24,28},{1,5},{5,9},{9,... | collective-permute-start | bytes 442376 | tf_op jit(solution)/shard_map/ppermute | solution.py:89
  65.7 6.3 %copy-start.2 = (bf16[1,2048,1024]{2,1,0:T(8,128)(2,1)S(1)}, bf16[1,2048,1024]{2,1,0:T(8,128)(2,1)}, u32[]{:S(2)}) copy-start(bf16[1,2048,1024]{2,1,0:T(8,128)(2,1)} %param.27) | copy-start | bytes 12582916
  65.7 6.3 %copy-start.4 = (bf16[768,2048]{1,0:T(8,128)(2,1)S(1)}, bf16[768,2048]{1,0:T(8,128)(2,1)}, u32[]{:S(2)}) copy-start(bf16[768,2048]{1,0:T(8,128)(2,1)} %all-gather.2.cloned.1.call-done) | copy-start | bytes 9437188
  72.0 3.8 %copy-start.3 = (bf16[1,2048,1024]{2,1,0:T(8,128)(2,1)S(1)}, bf16[1,2048,1024]{2,1,0:T(8,128)(2,1)}, u32[]{:S(2)}) copy-start(bf16[1,2048,1024]{2,1,0:T(8,128)(2,1)} %param.29) | copy-start | bytes 12582916
  80.8 66.9 %reduce-scatter.3.cloned.1.call-start = ((), (), s32[]{:S(2)}) async-start(), calls=%async_computation.5 | async-start | bytes 1310720 | tf_op jit(solution)/shard_map/reduce_scatter | solution.py:126
  80.8 6.9 %collective-permute-start.2 = (bf16[4,144,128]{2,1,0:T(8,128)(2,1)S(1)}, bf16[4,144,128]{2,1,0:T(8,128)(2,1)S(1)}, u32[]{:S(2)}, u32[]{:S(2)}) collective-permute-start(bf16[4,144,128]{2,1,0:T(8,128)(2,1)S(1)} %convert_element_type.34), channel_id=1, source_target_pairs={{0,8},{4,12},{8,16},{12,20},{16,24},{20,28},{1,9},{5,13},{9,17},{1... | collective-permute-start | bytes 442376 | tf_op jit(solution)/shard_map/ppermute | solution.py:89
  87.8 8.0 %collective-permute-start.3 = (bf16[4,144,128]{2,1,0:T(8,128)(2,1)S(1)}, bf16[4,144,128]{2,1,0:T(8,128)(2,1)S(1)}, u32[]{:S(2)}, u32[]{:S(2)}) collective-permute-start(bf16[4,144,128]{2,1,0:T(8,128)(2,1)S(1)} %get-tuple-element.16), channel_id=1, source_target_pairs={{0,16},{4,20},{8,24},{12,28},{1,17},{5,21},{9,25},{13,29},{2,18},{... | collective-permute-start | bytes 442376 | tf_op jit(solution)/shard_map/ppermute | solution.py:89
  96.7 27.4 %copy-start.1 = (f32[256,2]{0,1:T(2,128)S(1)}, f32[256,2]{0,1:T(2,128)}, u32[]{:S(2)}) copy-start(f32[256,2]{0,1:T(2,128)} %param.26) | copy-start | bytes 6148
  118.6 25.6 %all-to-all-start.1 = ((bf16[8,96,512]{2,1,0:T(8,128)(2,1)}), bf16[8,96,512]{2,1,0:T(8,128)(2,1)S(1)}, u32[]{:S(2)}, u32[]{:S(2)}) async-start(bf16[8,96,512]{2,1,0:T(8,128)(2,1)} %bitcast.30), calls=%async_computation.3 | async-start | bytes 1572864 | tf_op jit(solution)/shard_map/all_to_all | solution.py:178
  144.2 0.9 copy-start
Sparse Core Ops, SparseCore 0:
  38.1 27.5 all-gather.1
  80.9 37.7 reduce-scatter.4
  121.7 24.7 reduce-scatter.2
